TPU v7x, 32 devices: a whole 2x2x4 slice. The times are simulated.
32 devices in a mesh: sp: 8 (over z, core), tp: 4 (over y, x).
Axes of the slice: x: 2, y: 2, z: 4, core: 2. Of those that a mesh axis runs over, the one named last changes fastest.
Arguments:
- residual: bfloat16 [1024, 2048], P('sp', 'tp'), may hold values from -48 to 48
- glu_value: bfloat16 [1024, 2048], P('sp', 'tp'), may hold values from -48 to 48
- glu_gate: bfloat16 [1024, 2048], P('sp', 'tp'), may hold values from -6 to 6
- conv_weight: bfloat16 [31, 2048], P(None, 'tp'), may hold values from -1 to 1
- conv_bias: float32 [2048], P('tp'), may hold values from -3 to 3
- ln_gain: float32 [2048], P('tp'), may hold values from 0.1 to 1.9
- ln_bias: float32 [2048], P('tp'), may hold values from -3 to 3
- out_weight: bfloat16 [2048, 2048], P(None, 'tp'), may hold values from -0.125 to 0.125
- norm_gain: float32 [2048], P('tp'), may hold values from 0.1 to 1.9
- route_ids: int32 [1024, 2], P('sp'), may hold values from 0 to 7, all different within a row; in each aligned block of 128 rows (0 to 127, 128 to 255, ...) at most 64 rows name the same one
- route_weight: float32 [1024, 2], P('sp'), may hold values from 0.1 to 1
- expert_gate: bfloat16 [8, 2048, 4096], P('sp', None, 'tp'), may hold values from -0.125 to 0.125
- expert_up: bfloat16 [8, 2048, 4096], P('sp', None, 'tp'), may hold values from -0.125 to 0.125
- expert_down: bfloat16 [8, 4096, 2048], P('sp', 'tp'), may hold values from -0.09375 to 0.09375
Outputs:
- layer_out: bfloat16 [1024, 2048], P('sp', 'tp')
Inputs may be any that keep to these rules, and one draw needn't show every extreme that they name: `route_ids`: within the 128 rows of one index of sp, no expert is named more than 64 times, and in some such rows one expert is named exactly 64 times.
All inputs are finite; a program needn't handle non-finite values.
Results may differ from a plain program's by a relative error of at most 0.006.
Values may be sent and summed in bfloat16 or wider, within the bound.
A program may use at most 64 MiB of HBM per device.

v0:
```python
import jax
import jax.numpy as jnp
from jax import lax
from jax.sharding import PartitionSpec as P

TOPK = 2


def with_halo(cells, sides, width):
    for axis, dim in sides:
        count = lax.axis_size(axis)
        ends = count - 1
        head = lax.slice_in_dim(cells, 0, width, axis=dim)
        tail = lax.slice_in_dim(cells, cells.shape[dim] - width, cells.shape[dim], axis=dim)
        cells = jnp.concatenate(
            [
                lax.ppermute(tail, axis, [(i, (i + 1) % count) for i in range(ends)]),
                cells,
                lax.ppermute(head, axis, [((i + 1) % count, i) for i in range(ends)]),
            ],
            axis=dim,
        )
    return cells


def on_device(
    residual,
    glu_value,
    glu_gate,
    conv_weight,
    conv_bias,
    ln_gain,
    ln_bias,
    out_weight,
    norm_gain,
    route_ids,
    route_weight,
    expert_gate,
    expert_up,
    expert_down,
):
    rows = residual.shape[0]
    width_all = out_weight.shape[0]
    gated = (glu_value.astype(jnp.float32) * jax.nn.sigmoid(glu_gate.astype(jnp.float32))).astype(
        jnp.bfloat16
    )
    reach = conv_weight.shape[0] // 2
    padded = with_halo(gated, (("sp", 0),), reach)
    taps = conv_weight.astype(jnp.float32)
    conv = jnp.zeros(gated.shape, jnp.float32) + conv_bias
    for tap in range(conv_weight.shape[0]):
        conv = conv + padded[tap : tap + rows].astype(jnp.float32) * taps[tap]
    totals = lax.psum((jnp.sum(conv, axis=1), jnp.sum(conv * conv, axis=1)), "tp")
    mean = (totals[0] / width_all)[:, None]
    var = (totals[1] / width_all)[:, None] - mean * mean
    act = jax.nn.silu((conv - mean) * lax.rsqrt(var + 1e-05) * ln_gain + ln_bias).astype(
        jnp.bfloat16
    )
    projected = jnp.dot(
        lax.all_gather(act, "tp", axis=1, tiled=True),
        out_weight,
        preferred_element_type=jnp.float32,
    )
    mixed = residual.astype(jnp.float32) + projected
    squares = lax.psum(jnp.sum(mixed * mixed, axis=1), "tp")
    normed = (mixed * lax.rsqrt(squares / width_all + 1e-06)[:, None] * norm_gain).astype(
        jnp.bfloat16
    )
    experts = lax.axis_size("sp")
    capacity = 2 * rows * TOPK // experts
    flat = route_ids.reshape(-1)
    onehot = (flat[:, None] == jnp.arange(experts, dtype=jnp.int32)[None, :]).astype(jnp.int32)
    rank = jnp.sum((jnp.cumsum(onehot, axis=0) - 1) * onehot, axis=1)
    slot_of = flat * capacity + rank
    placing = (slot_of[None, :] == jnp.arange(experts * capacity, dtype=jnp.int32)[:, None]).astype(
        jnp.bfloat16
    )
    copies = jnp.repeat(normed, TOPK, axis=0)
    outgoing = jnp.dot(placing, copies, preferred_element_type=jnp.float32).astype(jnp.bfloat16)
    outgoing = outgoing.reshape(experts, capacity, normed.shape[1])
    arrived = lax.all_to_all(outgoing, "sp", split_axis=0, concat_axis=0, tiled=True)
    arrived = lax.all_gather(
        arrived.reshape(experts * capacity, normed.shape[1]), "tp", axis=1, tiled=True
    )
    gate = jnp.dot(arrived, expert_gate[0], preferred_element_type=jnp.float32)
    up = jnp.dot(arrived, expert_up[0], preferred_element_type=jnp.float32)
    hidden = (jax.nn.silu(gate) * up).astype(jnp.bfloat16)
    partial_out = jnp.dot(hidden, expert_down[0], preferred_element_type=jnp.float32)
    summed = lax.psum_scatter(
        partial_out.astype(jnp.bfloat16), "tp", scatter_dimension=1, tiled=True
    )
    summed = summed.reshape(experts, capacity, summed.shape[1])
    returned = lax.all_to_all(summed, "sp", split_axis=0, concat_axis=0, tiled=True)
    returned = returned.reshape(experts * capacity, returned.shape[2])
    picked = lax.dot_general(
        placing, returned, (((0,), (0,)), ((), ())), preferred_element_type=jnp.float32
    )
    picked = picked.reshape(rows, TOPK, picked.shape[1])
    moe = jnp.sum(picked * route_weight[:, :, None], axis=1)
    return (mixed + moe).astype(jnp.bfloat16)


def solution(mesh):
    in_specs = (
        P("sp", "tp"),
        P("sp", "tp"),
        P("sp", "tp"),
        P(None, "tp"),
        P("tp"),
        P("tp"),
        P("tp"),
        P(None, "tp"),
        P("tp"),
        P("sp", None),
        P("sp", None),
        P("sp", None, "tp"),
        P("sp", None, "tp"),
        P("sp", "tp", None),
    )
    out_specs = P("sp", "tp")
    return jax.shard_map(
        on_device, mesh=mesh, in_specs=in_specs, out_specs=out_specs, check_vma=False
    )
```

profile of v0, /device:TPU:0, one launch (start us, length us, event | category | flops | bytes accessed | tf_op | source)
XLA Modules:
  0.0 184.5 jit_solution(897781840962571341)
XLA Ops:
  6.5 0.0 copy-start
  6.5 0.0 copy-start.1
  6.5 0.0 all-gather.2.cloned.1.call-start
  6.5 1.2 multiply_convert_fusion.3
  7.8 2.4 %collective-permute-start = (bf16[15,512]{1,0:T(8,128)(2,1)S(1)}, bf16[15,512]{1,0:T(8,128)(2,1)S(1)}, u32[]{:S(2)}, u32[]{:S(2)}) collective-permute-start(bf16[15,512]{1,0:T(8,128)(2,1)S(1)} %get-tuple-element.10), channel_id=1, source_target_pairs={{0,4},{4,8},{8,12},{12,16},{16,20},{20,24},{24,28},{1,5},{5,9},{9,... | collective-permute-start | bytes 46088 | tf_op jit(solution)/shard_map/ppermute | solution.py:17
  10.2 1.3 collective-permute-start.1
  11.5 1.0 fusion.52
  12.4 1.0 fusion.51
  13.5 0.8 copy.20
  14.3 0.1 reshape.76
  14.4 0.1 eq.58
  14.6 0.6 reduce-window.6
  15.2 0.2 slice_reduce_fusion
  15.4 0.1 fusion.46
  15.5 0.0 collective-permute-done
  15.5 0.0 collective-permute-done.1
  15.5 2.0 %fusion.49 = (f32[128]{0:T(128)S(1)}, f32[128]{0:T(128)S(1)}, f32[128,512]{1,0:T(8,128)S(1)}) fusion(f32[512]{0:T(512)S(1)} %bitcast.82, bf16[15,512]{1,0:T(8,128)(2,1)S(1)} %collective-permute-done.1, bf16[128,512]{1,0:T(8,128)(2,1)S(1)} %multiply_convert_fusion.3, f32[512]{0:T(512)S(1)} %bitcast.81, f32[512]{0:T(512)S(1)} %bitcast.80, ...), kind=kLoop, calls=%fused_computation.114 | loop fusion | flops 12189440 | bytes 490496 | tf_op jit(solution)/shard_map/reduce_sum | solution.py:53
  17.5 0.0 copy-start.3
  17.5 10.7 %all-reduce = (f32[128]{0:T(128)S(1)}, f32[128]{0:T(128)S(1)}) all-reduce(f32[128]{0:T(128)S(1)} %get-tuple-element.6, f32[128]{0:T(128)S(1)} %get-tuple-element.5), channel_id=1, replica_groups=mesh['sp'=8,'tp'=4] {'tp'}, use_global_device_ids=true, to_apply=%region_3.0 | all-reduce | flops 256 | bytes 2048 | tf_op jit(solution)/shard_map/psum | solution.py:53
  28.3 0.9 multiply_convert_fusion.2
  29.2 9.6 %all_gather.6 = bf16[128,2048]{1,0:T(8,128)(2,1)S(1)} all-gather(bf16[128,512]{1,0:T(8,128)(2,1)S(1)} %multiply_convert_fusion.2), channel_id=1, replica_groups=mesh['sp'=8,'tp'=4] {'tp'}, dimensions={1}, use_global_device_ids=true | all-gather | bytes 655360 | tf_op jit(solution)/shard_map/all_gather | solution.py:60
  38.8 0.0 copy-done
  38.8 0.0 copy-done.1
  38.8 0.6 multiply_reduce_fusion
  39.3 8.9 %psum.23 = f32[128]{0:T(128)S(1)} all-reduce(f32[128]{0:T(128)S(1)} %get-tuple-element.45), channel_id=1, replica_groups=mesh['sp'=8,'tp'=4] {'tp'}, use_global_device_ids=true, to_apply=%region_8.9 | all-reduce | flops 128 | bytes 1024 | tf_op jit(solution)/shard_map/psum | solution.py:65
  48.3 0.0 copy-done.3
  48.3 0.1 multiply_convert_fusion.1
  48.4 0.1 broadcast_in_dim.2
  48.5 0.1 reshape.78
  48.7 0.3 convolution_convert_fusion
  49.0 22.2 %all_to_all.10 = bf16[8,64,512]{2,1,0:T(8,128)(2,1)} all-to-all(bf16[8,64,512]{2,1,0:T(8,128)(2,1)S(1)} %bitcast.68), channel_id=1, replica_groups=mesh['sp'=8,'tp'=4] {'sp'}, dimensions={0} | all-to-all | bytes 1048576 | tf_op jit(solution)/shard_map/all_to_all | solution.py:81
  71.2 0.0 all-gather.2.cloned.1.call-update
  71.2 0.0 reduce-scatter.2.cloned.1.call-start
  71.2 33.1 %all-gather.2.cloned.1.call-done = bf16[512,2048]{1,0:T(8,128)(2,1)} async-done(((bf16[512,512]{1,0:T(8,128)(2,1)}), bf16[512,2048]{1,0:T(8,128)(2,1)}) %all-gather.2.cloned.1.call-update) | async-done | bytes 2097168 | tf_op jit(solution)/shard_map/all_gather | solution.py:82
  104.3 6.5 %fusion.4 = f32[512,1024]{1,0:T(8,128)} fusion(bf16[512,2048]{1,0:T(8,128)(2,1)} %all-gather.2.cloned.1.call-done, bf16[1,2048,1024]{2,1,0:T(8,128)(2,1)} %param.25), kind=kOutput, calls=%fused_computation.4 | convolution fusion | flops 2147483648 | bytes 8388608 | tf_op jit(solution)/shard_map/dot_general | solution.py:85
  110.8 10.5 %fusion.6 = bf16[512,2048]{1,0:T(8,128)(2,1)} fusion(bf16[1,1024,2048]{2,1,0:T(8,128)(2,1)} %param.27, f32[512,1024]{1,0:T(8,128)} %fusion.4, bf16[512,2048]{1,0:T(8,128)(2,1)} %all-gather.2.cloned.1.call-done, bf16[1,2048,1024]{2,1,0:T(8,128)(2,1)} %param.26), kind=kOutput, calls=%fused_computation.6 | convolution fusion | flops 4299161600 | bytes 14680064 | tf_op jit(solution)/shard_map/dot_general | solution.py:88
  121.4 0.0 copy-start.2
  121.4 0.0 copy-start.4
  121.4 0.0 reduce-scatter.2.cloned.1.call-update
  121.4 35.3 %reduce-scatter.2.cloned.1.call-done = bf16[512,512]{1,0:T(8,128)(2,1)} async-done(((bf16[512,2048]{1,0:T(8,128)(2,1)}), bf16[512,512]{1,0:T(8,128)(2,1)}) %reduce-scatter.2.cloned.1.call-update) | async-done | bytes 524304 | tf_op jit(solution)/shard_map/reduce_scatter | solution.py:89
  156.7 4.6 %all-to-all-start.1 = ((bf16[8,64,512]{2,1,0:T(8,128)(2,1)}), bf16[8,64,512]{2,1,0:T(8,128)(2,1)S(1)}, u32[]{:S(2)}, u32[]{:S(2)}) async-start(bf16[8,64,512]{2,1,0:T(8,128)(2,1)} %bitcast.69), calls=%async_computation.2 | async-start | bytes 1048576 | tf_op jit(solution)/shard_map/all_to_all | solution.py:93
  161.3 0.1 reduce_sum.50
  161.5 0.1 copy.22
  161.5 0.0 copy-done.2
  161.5 15.1 %all-to-all-done.1 = bf16[8,64,512]{2,1,0:T(8,128)(2,1)S(1)} async-done(((bf16[8,64,512]{2,1,0:T(8,128)(2,1)}), bf16[8,64,512]{2,1,0:T(8,128)(2,1)S(1)}, u32[]{:S(2)}, u32[]{:S(2)}) %all-to-all-start.1) | async-done | bytes 524320 | tf_op jit(solution)/shard_map/all_to_all | solution.py:93
  176.7 0.0 copy-done.4
  176.7 0.3 fusion.11
  177.0 0.7 add_convert_fusion
  (8 shorter events, 0.1 us)
Async XLA Ops:
  6.5 32.2 %copy-start = (bf16[2048,512]{1,0:T(8,128)(2,1)S(1)}, bf16[2048,512]{1,0:T(8,128)(2,1)}, u32[]{:S(2)}) copy-start(bf16[2048,512]{1,0:T(8,128)(2,1)} %param.21) | copy-start | bytes 6291460
  6.5 32.2 %copy-start.1 = (bf16[128,512]{1,0:T(8,128)(2,1)S(1)}, bf16[128,512]{1,0:T(8,128)(2,1)}, u32[]{:S(2)}) copy-start(bf16[128,512]{1,0:T(8,128)(2,1)} %param.14) | copy-start | bytes 393220
  6.5 97.8 %all-gather.2.cloned.1.call-start = ((), (), s32[]{:S(2)}) async-start(), calls=%async_computation.3 | async-start | bytes 2621440 | tf_op jit(solution)/shard_map/all_gather | solution.py:82
  7.8 7.8 %collective-permute-start = (bf16[15,512]{1,0:T(8,128)(2,1)S(1)}, bf16[15,512]{1,0:T(8,128)(2,1)S(1)}, u32[]{:S(2)}, u32[]{:S(2)}) collective-permute-start(bf16[15,512]{1,0:T(8,128)(2,1)S(1)} %get-tuple-element.10), channel_id=1, source_target_pairs={{0,4},{4,8},{8,12},{12,16},{16,20},{20,24},{24,28},{1,5},{5,9},{9,... | collective-permute-start | bytes 46088 | tf_op jit(solution)/shard_map/ppermute | solution.py:17
  10.2 5.4 %collective-permute-start.1 = (bf16[15,512]{1,0:T(8,128)(2,1)S(1)}, bf16[15,512]{1,0:T(8,128)(2,1)S(1)}, u32[]{:S(2)}, u32[]{:S(2)}) collective-permute-start(bf16[15,512]{1,0:T(8,128)(2,1)S(1)} %get-tuple-element.11), channel_id=1, source_target_pairs={{4,0},{8,4},{12,8},{16,12},{20,16},{24,20},{28,24},{5,1},{9,5},{13... | collective-permute-start | bytes 46088 | tf_op jit(solution)/shard_map/ppermute | solution.py:19
  17.5 30.8 %copy-start.3 = (f32[512]{0:T(512)S(1)}, f32[512]{0:T(512)}, u32[]{:S(2)}) copy-start(f32[512]{0:T(512)} %param.22) | copy-start | bytes 6148
  71.2 85.5 %reduce-scatter.2.cloned.1.call-start = ((), (), s32[]{:S(2)}) async-start(), calls=%async_computation.4 | async-start | bytes 2621440 | tf_op jit(solution)/shard_map/reduce_scatter | solution.py:89
  121.4 40.2 %copy-start.2 = (s32[128,2]{0,1:T(2,128)S(1)}, s32[128,2]{0,1:T(2,128)}, u32[]{:S(2)}) copy-start(s32[128,2]{0,1:T(2,128)} %param.23) | copy-start | bytes 3076
  121.4 55.3 %copy-start.4 = (f32[128,2]{0,1:T(2,128)S(1)}, f32[128,2]{0,1:T(2,128)}, u32[]{:S(2)}) copy-start(f32[128,2]{0,1:T(2,128)} %param.24) | copy-start | bytes 3076
  156.7 19.9 %all-to-all-start.1 = ((bf16[8,64,512]{2,1,0:T(8,128)(2,1)}), bf16[8,64,512]{2,1,0:T(8,128)(2,1)S(1)}, u32[]{:S(2)}, u32[]{:S(2)}) async-start(bf16[8,64,512]{2,1,0:T(8,128)(2,1)} %bitcast.69), calls=%async_computation.2 | async-start | bytes 1048576 | tf_op jit(solution)/shard_map/all_to_all | solution.py:93
Sparse Core Ops, SparseCore 0:
  71.3 32.9 all-gather.1
  121.5 35.1 reduce-scatter.1
where the time goes:
time: 185 us
  waiting for transfers between devices  83.6 us (45%)
  blocking collectives  51.5 us (28%)
  matrix products  18.2 us (10%)
  between operations  13.6 us (7%)
  starting transfers between devices  8.34 us (5%)
  other arithmetic  5.59 us (3%)
  local copies, waits for them, and re-layouts  3.76 us (2%)
    reduce_scatter x1, waiting for transfers between devices, on_device(): lax.psum_scatter(partial_out.astype(jnp.bfloat16), 'tp', scatter_dimensio...  35.3 us
    all_gather x1, waiting for transfers between devices, on_device(): lax.all_gather(arrived.reshape(experts * capacity, normed.shape[1]), 'tp'...  33.1 us
    all_to_all x1, blocking collectives, on_device(): lax.all_to_all(outgoing, 'sp', split_axis=0, concat_axis=0, tiled=True)  22.2 us
    all_to_all x1, waiting for transfers between devices, on_device(): lax.all_to_all(summed, 'sp', split_axis=0, concat_axis=0, tiled=True)  15.1 us
    psum x1, blocking collectives, on_device(): lax.psum((jnp.sum(conv, axis=1), jnp.sum(conv * conv, axis=1)), 'tp')  10.7 us
    dot_general x1, matrix products, on_device(): jnp.dot(hidden, expert_down[0], preferred_element_type=jnp.float32)  10.5 us
    all_gather x1, blocking collectives, on_device(): lax.all_gather(act, 'tp', axis=1, tiled=True)  9.61 us
    psum x1, blocking collectives, on_device(): squares = lax.psum(jnp.sum(mixed * mixed, axis=1), 'tp')  8.93 us
  transfers between devices with their start and end apart: 5, of which 3 were waited for; matrix products, arithmetic and copies ran while one was open for 2% of the time, Pallas kernels for 0%

commit v1 on v0

--- a/solution.py
+++ b/solution.py
@@ -1,6 +1,10 @@
+import functools
+
 import jax
 import jax.numpy as jnp
 from jax import lax
+from jax.experimental import pallas as pl
+from jax.experimental.pallas import tpu as pltpu
 from jax.sharding import PartitionSpec as P
 
 TOPK = 2
@@ -100,6 +104,392 @@
     return (mixed + moe).astype(jnp.bfloat16)
 
 
+F32 = jnp.float32
+BF16 = jnp.bfloat16
+GROUPS = 4
+
+
+def dot(a, b):
+    return jnp.dot(a, b, preferred_element_type=F32)
+
+
+def layer_kernel(
+    nsp, ntp,
+    res_ref, val_ref, gate_ref, cw_ref, cb_ref, lg_ref, lb_ref, ng_ref, ids_ref, rw_ref,
+    ow_hbm, eg_hbm, eu_hbm, ed_hbm,
+    out_ref,
+    ow, wg, wu, wd, pad, wf, conv, mixed, halo_out, halo_in, st_out, st_in,
+    act, outgoing, arr, hid, part, one, two_out, two, fin, ret,
+    w_sem, halo_s, halo_r, st_s, st_r, ag_s, ag_r, zs_s, zs_r, x_s, x_r, r_s, r_r, h_s, h_r,
+):
+    rows, ch = res_ref.shape
+    width = ow.shape[0]
+    taps = cw_ref.shape[0]
+    reach = taps // 2
+    edge = halo_in.shape[1]
+    size = nsp // GROUPS
+    cap = outgoing.shape[0] // nsp
+    grp = size * cap
+    half = grp // 2
+    me = lax.axis_index("sp")
+    t = lax.axis_index("tp")
+    gi, mi = me // size, me % size
+    cx, cy = t % 2, t // 2
+    tx = cy * 2 + 1 - cx
+    ty = (1 - cy) * 2 + cx
+    td = (1 - cy) * 2 + 1 - cx
+
+    def remote(src, dst, ss, rs, **dev):
+        return pltpu.make_async_remote_copy(
+            src_ref=src, dst_ref=dst, send_sem=ss, recv_sem=rs,
+            device_id=dev, device_id_type=pl.DeviceIdType.MESH,
+        )
+
+    barrier = pltpu.get_barrier_semaphore()
+    for d in range(1, ntp):
+        pl.semaphore_signal(barrier, inc=1, device_id={"tp": (t + d) % ntp},
+                            device_id_type=pl.DeviceIdType.MESH)
+    for d in range(1, nsp):
+        pl.semaphore_signal(barrier, inc=1, device_id={"sp": (me + d) % nsp},
+                            device_id_type=pl.DeviceIdType.MESH)
+    loads = [
+        pltpu.make_async_copy(ow_hbm, ow, w_sem.at[0]),
+        pltpu.make_async_copy(eg_hbm.at[0], wg, w_sem.at[1]),
+        pltpu.make_async_copy(eu_hbm.at[0], wu, w_sem.at[2]),
+        pltpu.make_async_copy(ed_hbm.at[0], wd, w_sem.at[3]),
+    ]
+    for load in loads:
+        load.start()
+
+    gated = (val_ref[...].astype(F32) * jax.nn.sigmoid(gate_ref[...].astype(F32))).astype(BF16)
+    halo_out[0] = gated[rows - edge:]
+    halo_out[1] = gated[:edge]
+    pad[edge:edge + rows, :] = gated.astype(F32)
+    pad[0:edge, :] = jnp.zeros((edge, ch), F32)
+    pad[edge + rows:, :] = jnp.zeros((edge, ch), F32)
+    wf[0:taps, :] = cw_ref[...].astype(F32)
+    pl.semaphore_wait(barrier, ntp + nsp - 2)
+    to_right = remote(halo_out.at[0], halo_in.at[0], halo_s.at[0], halo_r.at[0], sp=(me + 1) % nsp)
+    to_left = remote(halo_out.at[1], halo_in.at[1], halo_s.at[1], halo_r.at[1],
+                     sp=(me + nsp - 1) % nsp)
+
+    @pl.when(me < nsp - 1)
+    def _():
+        to_right.start()
+
+    @pl.when(me > 0)
+    def _():
+        to_left.start()
+
+    lane = lax.broadcasted_iota(jnp.int32, (rows, 128), 1)
+    row = lax.broadcasted_iota(jnp.int32, (rows, rows), 0)
+    col = lax.broadcasted_iota(jnp.int32, (rows, rows), 1)
+    id0, id1 = ids_ref[:, 0:1], ids_ref[:, 1:2]
+    hit0, hit1 = lane == id0, lane == id1
+    named = jnp.where(hit0, 1.0, jnp.where(hit1, 1.0, 0.0)).astype(BF16)
+    before = jnp.where(col < row, 1.0, 0.0).astype(BF16)
+    rank = dot(before, named)
+    rank0 = jnp.sum(jnp.where(hit0, rank, 0.0), axis=1, keepdims=True).astype(jnp.int32)
+    rank1 = jnp.sum(jnp.where(hit1, rank, 0.0), axis=1, keepdims=True).astype(jnp.int32)
+    slot = lax.broadcasted_iota(jnp.int32, (rows, nsp * cap), 1)
+    pick0 = jnp.where(slot == id0 * cap + rank0, 1.0, 0.0)
+    pick1 = jnp.where(slot == id1 * cap + rank1, 1.0, 0.0)
+    placing = (pick0 + pick1).T.astype(BF16)
+    pick0 = pick0.astype(BF16)
+    pick1 = pick1.astype(BF16)
+
+    @pl.when(me > 0)
+    def _():
+        to_right.wait_recv()
+        pad[0:edge, :] = halo_in[0].astype(F32)
+
+    @pl.when(me < nsp - 1)
+    def _():
+        to_left.wait_recv()
+        pad[edge + rows:, :] = halo_in[1].astype(F32)
+
+    for j in range(0, ch, 128):
+        total = jnp.zeros((rows, 128), F32) + cb_ref[:, j:j + 128]
+        for tap in range(taps):
+            at = tap + edge - reach
+            total = total + pad[at:at + rows, j:j + 128] * wf[tap:tap + 1, j:j + 128]
+        conv[:, j:j + 128] = total
+
+    def row_totals(which, sums):
+        block = jnp.zeros((rows, 128), F32)
+        for n, s in enumerate(sums):
+            block = jnp.where(lane == n, s, block)
+        mine = block.T[0:8, :]
+        st_out[which] = mine
+        copies = []
+        for d in range(1, ntp):
+            n = which * ntp + d
+            copy = remote(st_out.at[which], st_in.at[which, d], st_s.at[n], st_r.at[n],
+                          tp=(t + d) % ntp)
+            copy.start()
+            copies.append(copy)
+        total = mine
+        for d, copy in enumerate(copies):
+            copy.wait_recv()
+            total = total + st_in[which, d + 1]
+        back = jnp.concatenate([total, jnp.zeros((rows - 8, 128), F32)], axis=0).T
+        return [back[:, n:n + 1] for n in range(len(sums))], copies
+
+    c = conv[...]
+    (s1, s2), st1 = row_totals(
+        0, (jnp.sum(c, axis=1, keepdims=True), jnp.sum(c * c, axis=1, keepdims=True))
+    )
+    mean = s1 / width
+    var = s2 / width - mean * mean
+    act[t] = jax.nn.silu(
+        (conv[...] - mean) * lax.rsqrt(var + 1e-05) * lg_ref[...] + lb_ref[...]
+    ).astype(BF16)
+
+    mid = rows // 2
+    ag = [
+        remote(act.at[t], act.at[t], ag_s.at[0], ag_r.at[0], tp=tx),
+        remote(act.at[t], act.at[t], ag_s.at[1], ag_r.at[1], tp=ty),
+        remote(act.at[tx, pl.ds(0, mid)], act.at[tx, pl.ds(0, mid)], ag_s.at[2], ag_r.at[2], tp=ty),
+        remote(act.at[ty, pl.ds(mid, mid)], act.at[ty, pl.ds(mid, mid)], ag_s.at[3], ag_r.at[3],
+               tp=tx),
+    ]
+
+    def arrival(n, block):
+        return remote(block, block, ag_s.at[n], ag_r.at[n], tp=tx)
+
+    def columns(of):
+        return ow[pl.ds(pl.multiple_of(of * ch, ch), ch), :]
+
+    ag[0].start()
+    ag[1].start()
+    loads[0].wait()
+    mixed[...] = res_ref[...].astype(F32) + dot(act[t], columns(t))
+    arrival(0, act.at[tx]).wait_recv()
+    ag[2].start()
+    arrival(1, act.at[ty]).wait_recv()
+    ag[3].start()
+    mixed[...] += dot(act[tx], columns(tx)) + dot(act[ty], columns(ty))
+    arrival(2, act.at[td, pl.ds(0, mid)]).wait_recv()
+    arrival(3, act.at[td, pl.ds(mid, mid)]).wait_recv()
+    full = mixed[...] + dot(act[td], columns(td))
+    mixed[...] = full
+    (sq,), st2 = row_totals(1, (jnp.sum(full * full, axis=1, keepdims=True),))
+    normed = (mixed[...] * lax.rsqrt(sq / width + 1e-06) * ng_ref[...]).astype(BF16)
+    outgoing[...] = dot(placing, normed).astype(BF16)
+
+    def piece(n):
+        return pl.ds(pl.multiple_of(n * cap, cap), cap)
+
+    zs = []
+    for k in range(GROUPS):
+        for i in range(size):
+            if k == 0 and i == 0:
+                continue
+            e = (gi - k + GROUPS) % GROUPS * size + (mi + i) % size
+            place = k * size + mi
+            copy = remote(outgoing.at[piece(e)], arr.at[t, piece(place)],
+                          zs_s.at[k * size + i], zs_r.at[place], sp=e)
+            copy.start()
+            zs.append(copy)
+    arr[t, piece(mi), :] = outgoing[piece(me), :]
+
+    pending = []
+
+    def send(copy):
+        copy.start()
+        pending.append(copy)
+
+    def span(k):
+        return pl.ds(k * grp, grp)
+
+    def front(k):
+        return pl.ds(k * grp, half)
+
+    def rear(k):
+        return pl.ds(k * grp + half, half)
+
+    def share(k):
+        for i in range(size):
+            if k == 0 and i == 0:
+                continue
+            place = k * size + (mi + i) % size
+            remote(outgoing.at[piece(0)], arr.at[t, piece(place)], zs_s.at[0], zs_r.at[place],
+                   sp=me).wait_recv()
+        own = arr.at[t, span(k)]
+        send(remote(own, own, x_s.at[4 * k], x_r.at[4 * k], tp=tx))
+        send(remote(own, own, x_s.at[4 * k + 1], x_r.at[4 * k + 1], tp=ty))
+
+    def landed(n, block):
+        remote(block, block, x_s.at[n], x_r.at[n], tp=tx).wait_recv()
+
+    def relay(k):
+        landed(4 * k, arr.at[tx, span(k)])
+        block = arr.at[tx, front(k)]
+        send(remote(block, block, x_s.at[4 * k + 2], x_r.at[4 * k + 2], tp=ty))
+        landed(4 * k + 1, arr.at[ty, span(k)])
+        block = arr.at[ty, rear(k)]
+        send(remote(block, block, x_s.at[4 * k + 3], x_r.at[4 * k + 3], tp=tx))
+
+    def gather_end(k):
+        landed(4 * k + 2, arr.at[td, front(k)])
+        landed(4 * k + 3, arr.at[td, rear(k)])
+
+    inner = wg.shape[1]
+    tile = min(256, inner)
+
+    def experts(k):
+        def up(n, carry):
+            at = pl.ds(pl.multiple_of(n * tile, tile), tile)
+            g = jnp.zeros((grp, tile), F32)
+            u = jnp.zeros((grp, tile), F32)
+            for b in range(ntp):
+                x = arr[b, k * grp:(k + 1) * grp, :]
+                g = g + dot(x, wg[b * ch:(b + 1) * ch, at])
+                u = u + dot(x, wu[b * ch:(b + 1) * ch, at])
+            hid[:, at] = (jax.nn.silu(g) * u).astype(BF16)
+            return carry
+
+        def down(b, carry):
+            at = pl.ds(pl.multiple_of(b * ch, ch), ch)
+            part[b, k * grp:(k + 1) * grp, :] = dot(hid[...], wd[:, at]).astype(BF16)
+            return carry
+
+        if k == 0:
+            loads[1].wait()
+            loads[2].wait()
+        lax.fori_loop(0, inner // tile, up, 0)
+        if k == 0:
+            loads[3].wait()
+        lax.fori_loop(0, ntp, down, 0)
+        n = 6 * k
+        first = [
+            (part.at[tx, front(k)], one.at[0, front(k)], n, tx),
+            (part.at[td, front(k)], one.at[1, front(k)], n + 1, tx),
+            (part.at[ty, rear(k)], one.at[0, rear(k)], n + 2, ty),
+            (part.at[td, rear(k)], one.at[1, rear(k)], n + 3, ty),
+        ]
+        for src, dst, m, to in (first[1], first[3], first[0], first[2]):
+            send(remote(src, dst, r_s.at[m], r_r.at[m], tp=to))
+
+    def summed(m, block):
+        remote(block, block, r_s.at[m], r_r.at[m], tp=tx).wait_recv()
+
+    def reduce_mid(k):
+        n = 6 * k
+        for m, at, to in ((n + 1, front(k), ty), (n + 3, rear(k), tx)):
+            summed(m, one.at[1, at])
+            two_out[at, :] = (part[to, at, :].astype(F32) + one[1, at, :].astype(F32)).astype(BF16)
+            m2 = n + 4 + (m - n) // 2
+            send(remote(two_out.at[at], two.at[at], r_s.at[m2], r_r.at[m2], tp=to))
+
+    def reduce_end(k):
+        n = 6 * k
+        summed(n, one.at[0, front(k)])
+        summed(n + 2, one.at[0, rear(k)])
+        summed(n + 4, two.at[front(k)])
+        summed(n + 5, two.at[rear(k)])
+        at = span(k)
+        fin[at, :] = (
+            part[t, at, :].astype(F32) + one[0, at, :].astype(F32) + two[at, :].astype(F32)
+        ).astype(BF16)
+        for i in range(size):
+            if k == 0 and i == 0:
+                ret[piece(me), :] = fin[piece(mi), :]
+                continue
+            who = (mi + i) % size
+            home = (gi + k) % GROUPS * size + who
+            send(remote(fin.at[piece(k * size + who)], ret.at[piece(me)],
+                        h_s.at[k * size + i], h_r.at[me], sp=home))
+
+    for k in range(GROUPS):
+        if k == 0:
+            share(0)
+            share(1)
+        relay(k)
+        if 0 < k < GROUPS - 1:
+            share(k + 1)
+        gather_end(k)
+        experts(k)
+        if k >= 1:
+            reduce_mid(k - 1)
+        if k >= 2:
+            reduce_end(k - 2)
+    reduce_end(GROUPS - 2)
+    reduce_mid(GROUPS - 1)
+    reduce_end(GROUPS - 1)
+
+    for d in range(1, nsp):
+        e = (me + d) % nsp
+        remote(fin.at[piece(0)], ret.at[piece(e)], h_s.at[0], h_r.at[e], sp=me).wait_recv()
+    back = ret[...]
+    moe = dot(pick0, back) * rw_ref[:, 0:1] + dot(pick1, back) * rw_ref[:, 1:2]
+    out_ref[...] = (mixed[...] + moe).astype(out_ref.dtype)
+
+    @pl.when(me < nsp - 1)
+    def _():
+        to_right.wait_send()
+
+    @pl.when(me > 0)
+    def _():
+        to_left.wait_send()
+
+    for copy in st1 + st2 + ag + zs + pending:
+        copy.wait_send()
+
+
+def fused(nsp, ntp, *args):
+    (residual, glu_value, glu_gate, conv_weight, conv_bias, ln_gain, ln_bias, out_weight,
+     norm_gain, route_ids, route_weight, expert_gate, expert_up, expert_down) = args
+    rows, ch = residual.shape
+    width = out_weight.shape[0]
+    inner = expert_gate.shape[2]
+    cap = 2 * rows * TOPK // nsp
+    slots = nsp * cap
+    grp = slots // GROUPS
+    edge = -(-(conv_weight.shape[0] // 2) // 16) * 16
+    vmem = pl.BlockSpec(memory_space=pltpu.VMEM)
+    hbm = pl.BlockSpec(memory_space=pl.ANY)
+    dma = lambda n: pltpu.SemaphoreType.DMA((n,))
+    return pl.pallas_call(
+        functools.partial(layer_kernel, nsp, ntp),
+        out_shape=jax.ShapeDtypeStruct((rows, ch), residual.dtype),
+        in_specs=[vmem] * 10 + [hbm] * 4,
+        out_specs=vmem,
+        scratch_shapes=[
+            pltpu.VMEM((width, ch), BF16),
+            pltpu.VMEM((width, inner), BF16),
+            pltpu.VMEM((width, inner), BF16),
+            pltpu.VMEM((inner, width), BF16),
+            pltpu.VMEM((rows + 2 * edge, ch), F32),
+            pltpu.VMEM((-(-conv_weight.shape[0] // 8) * 8, ch), F32),
+            pltpu.VMEM((rows, ch), F32),
+            pltpu.VMEM((rows, ch), F32),
+            pltpu.VMEM((2, edge, ch), BF16),
+            pltpu.VMEM((2, edge, ch), BF16),
+            pltpu.VMEM((2, 8, 128), F32),
+            pltpu.VMEM((2, ntp, 8, 128), F32),
+            pltpu.VMEM((ntp, rows, ch), BF16),
+            pltpu.VMEM((slots, ch), BF16),
+            pltpu.VMEM((ntp, slots, ch), BF16),
+            pltpu.VMEM((grp, inner), BF16),
+            pltpu.VMEM((ntp, slots, ch), BF16),
+            pltpu.VMEM((2, slots, ch), BF16),
+            pltpu.VMEM((slots, ch), BF16),
+            pltpu.VMEM((slots, ch), BF16),
+            pltpu.VMEM((slots, ch), BF16),
+            pltpu.VMEM((slots, ch), BF16),
+            dma(4), dma(2), dma(2), dma(2 * ntp), dma(2 * ntp), dma(4), dma(4),
+            dma(nsp), dma(nsp), dma(4 * GROUPS), dma(4 * GROUPS), dma(6 * GROUPS),
+            dma(6 * GROUPS), dma(nsp), dma(nsp),
+        ],
+        compiler_params=pltpu.CompilerParams(
+            collective_id=0, has_side_effects=True, vmem_limit_bytes=52 * 1024 * 1024
+        ),
+    )(residual, glu_value, glu_gate, conv_weight, conv_bias.reshape(1, ch), ln_gain.reshape(1, ch),
+      ln_bias.reshape(1, ch), norm_gain.reshape(1, ch), route_ids, route_weight,
+      out_weight, expert_gate, expert_up, expert_down)
+
+
 def solution(mesh):
     in_specs = (
         P("sp", "tp"),
@@ -118,6 +508,10 @@
         P("sp", "tp", None),
     )
     out_specs = P("sp", "tp")
+    nsp, ntp = mesh.shape["sp"], mesh.shape["tp"]
+    body = on_device
+    if ntp == 4 and nsp % GROUPS == 0:
+        body = functools.partial(fused, nsp, ntp)
     return jax.shard_map(
-        on_device, mesh=mesh, in_specs=in_specs, out_specs=out_specs, check_vma=False
-    )
+        body, mesh=mesh, in_specs=in_specs, out_specs=out_specs, check_vma=False
+    )

time: 185 us -> 91.9 us (0.50)
  waiting for transfers between devices: 83.6 us -> 0 us
  Pallas kernels: 0 us -> 82.9 us
  blocking collectives: 51.5 us -> 0 us
  matrix products: 18.2 us -> 0 us
  between operations: 13.6 us -> 0.02 us
  starting transfers between devices: 8.34 us -> 0 us
  other arithmetic: 5.59 us -> 0 us
  local copies, waits for them, and re-layouts: 3.76 us -> 8.41 us
    pallas_call x0 -> x1, Pallas kernels: none -> 82.9 us  [fused(): pl.pallas_call(functools.partial(layer_kernel, nsp, ntp), out_shape=jax.S...]
    reduce_scatter x1 -> x0, waiting for transfers between devices: 35.3 us -> none  [on_device(): lax.psum_scatter(partial_out.astype(jnp.bfloat16), 'tp', scatter_dimensio...]
    all_gather x1 -> x0, waiting for transfers between devices: 33.1 us -> none  [on_device(): lax.all_gather(arrived.reshape(experts * capacity, normed.shape[1]), 'tp'...]
    all_to_all x1 -> x0, blocking collectives: 22.2 us -> none  [on_device(): lax.all_to_all(outgoing, 'sp', split_axis=0, concat_axis=0, tiled=True)]
    psum x2 -> x0, blocking collectives: 19.7 us -> none  [the longest x1 10.7 us: on_device(): lax.psum((jnp.sum(conv, axis=1), jnp.sum(conv * conv, axis=1)), 'tp')]
    dot_general x5 -> x0, matrix products: 18.2 us -> none  [the longest x1 10.5 us: on_device(): jnp.dot(hidden, expert_down[0], preferred_element_type=jnp.float32)]
    all_to_all x1 -> x0, waiting for transfers between devices: 15.1 us -> none  [on_device(): lax.all_to_all(summed, 'sp', split_axis=0, concat_axis=0, tiled=True)]
    all_gather x1 -> x0, blocking collectives: 9.61 us -> none  [on_device(): lax.all_gather(act, 'tp', axis=1, tiled=True)]
  transfers between devices with their start and end apart: 5 -> 0, of which waited for: 3 -> 0; matrix products, arithmetic and copies ran while one was open for 2% -> 0% of each run, Pallas kernels for 0% -> 0%
where the time goes in v1:
time: 91.9 us; the launch traced here: 91.3 us
  Pallas kernels  82.9 us (90%)
  local copies, waits for them, and re-layouts  8.41 us (9%)
    pallas_call x1, Pallas kernels, fused(): pl.pallas_call(functools.partial(layer_kernel, nsp, ntp), out_shape=jax.S...  82.9 us
    unnamed x19, local copies, waits for them, and re-layouts  8.41 us

profile of v1, /device:TPU:0, one launch (start us, length us, event | category | flops | bytes accessed | tf_op | source)
XLA Modules:
  0.0 91.3 jit_solution(16198094591147427771)
XLA Ops:
  0.0 0.8 copy.15.ids_ref
  0.8 0.8 copy.16.rw_ref
  1.6 0.0 copy-start
  1.6 0.9 copy-done
  2.5 0.0 copy-start.1
  2.5 0.9 copy-done.1
  3.4 0.0 copy-start.2
  3.4 0.9 copy-done.2
  4.3 0.0 copy-start.3
  4.3 0.8 copy-done.3
  5.0 0.0 copy-start.4
  5.0 0.7 copy-done.4
  5.7 0.0 copy-start.5
  5.7 0.7 copy-done.5
  6.4 0.0 copy-start.6
  6.4 0.7 copy-done.6
  7.1 0.0 copy-start.7
  7.1 0.7 copy-done.7
  7.8 82.9 %shard_map.136 = bf16[128,512]{1,0:T(8,128)(2,1)S(1)} custom-call(bf16[128,512]{1,0:T(8,128)(2,1)S(1)} %copy-done, bf16[128,512]{1,0:T(8,128)(2,1)S(1)} %copy-done.1, bf16[128,512]{1,0:T(8,128)(2,1)S(1)} %copy-done.2, bf16[31,512]{1,0:T(8,128)(2,1)S(1)} %copy-done.3, f32[1,512]{1,0:T(1,128)S(1)} %bitcast.4, f32[1,512]{1,0:T(1,128)S(1)} %bitcast.5, ...), custom_call_target="tpu_custom_call" | custom-call | tf_op jit(solution)/shard_map/pallas_call | solution.py:453
  90.7 0.7 copy.18
Async XLA Ops:
  1.6 0.9 copy-start
  2.5 0.9 copy-start.1
  3.4 0.9 copy-start.2
  4.3 0.8 copy-start.3
  5.0 0.7 copy-start.4
  5.7 0.7 copy-start.5
  6.4 0.7 copy-start.6
  7.1 0.7 copy-start.7

commit v2 on v1

--- a/solution.py
+++ b/solution.py
@@ -115,9 +115,10 @@
 
 def layer_kernel(
     nsp, ntp,
-    res_ref, val_ref, gate_ref, cw_ref, cb_ref, lg_ref, lb_ref, ng_ref, ids_ref, rw_ref,
+    res_hbm, val_hbm, gate_hbm, cw_hbm, cb_hbm, lg_hbm, lb_hbm, ng_hbm, ids_hbm, rw_hbm,
     ow_hbm, eg_hbm, eu_hbm, ed_hbm,
     out_ref,
+    res_ref, val_ref, gate_ref, cw_ref, cb_ref, lg_ref, lb_ref, ng_ref, ids_ref, rw_ref,
     ow, wg, wu, wd, pad, wf, conv, mixed, halo_out, halo_in, st_out, st_in,
     act, outgoing, arr, hid, part, one, two_out, two, fin, ret,
     w_sem, halo_s, halo_r, st_s, st_r, ag_s, ag_r, zs_s, zs_r, x_s, x_r, r_s, r_r, h_s, h_r,
@@ -145,6 +146,14 @@
             device_id=dev, device_id_type=pl.DeviceIdType.MESH,
         )
 
+    smalls = [
+        (val_hbm, val_ref), (gate_hbm, gate_ref), (cw_hbm, cw_ref), (cb_hbm, cb_ref),
+        (ids_hbm, ids_ref), (lg_hbm, lg_ref), (lb_hbm, lb_ref), (res_hbm, res_ref),
+        (ng_hbm, ng_ref), (rw_hbm, rw_ref),
+    ]
+    staged = [pltpu.make_async_copy(a, b, w_sem.at[4 + n]) for n, (a, b) in enumerate(smalls)]
+    for load in staged:
+        load.start()
     barrier = pltpu.get_barrier_semaphore()
     for d in range(1, ntp):
         pl.semaphore_signal(barrier, inc=1, device_id={"tp": (t + d) % ntp},
@@ -161,12 +170,15 @@
     for load in loads:
         load.start()
 
+    staged[0].wait()
+    staged[1].wait()
     gated = (val_ref[...].astype(F32) * jax.nn.sigmoid(gate_ref[...].astype(F32))).astype(BF16)
     halo_out[0] = gated[rows - edge:]
     halo_out[1] = gated[:edge]
     pad[edge:edge + rows, :] = gated.astype(F32)
     pad[0:edge, :] = jnp.zeros((edge, ch), F32)
     pad[edge + rows:, :] = jnp.zeros((edge, ch), F32)
+    staged[2].wait()
     wf[0:taps, :] = cw_ref[...].astype(F32)
     pl.semaphore_wait(barrier, ntp + nsp - 2)
     to_right = remote(halo_out.at[0], halo_in.at[0], halo_s.at[0], halo_r.at[0], sp=(me + 1) % nsp)
@@ -184,7 +196,16 @@
     lane = lax.broadcasted_iota(jnp.int32, (rows, 128), 1)
     row = lax.broadcasted_iota(jnp.int32, (rows, rows), 0)
     col = lax.broadcasted_iota(jnp.int32, (rows, rows), 1)
-    id0, id1 = ids_ref[:, 0:1], ids_ref[:, 1:2]
+    for load in staged[3:]:
+        load.wait()
+    topk = ids_ref.shape[0]
+
+    def upright(pair):
+        return jnp.concatenate([pair, jnp.zeros((128 - topk, rows), F32)], axis=0).T
+
+    ids = upright(ids_ref[...].astype(F32)).astype(jnp.int32)
+    id0, id1 = ids[:, 0:1], ids[:, 1:2]
+    weights = upright(rw_ref[...])
     hit0, hit1 = lane == id0, lane == id1
     named = jnp.where(hit0, 1.0, jnp.where(hit1, 1.0, 0.0)).astype(BF16)
     before = jnp.where(col < row, 1.0, 0.0).astype(BF16)
@@ -246,12 +267,12 @@
     ).astype(BF16)
 
     mid = rows // 2
+    low, high = pl.ds(0, mid), pl.ds(mid, mid)
     ag = [
-        remote(act.at[t], act.at[t], ag_s.at[0], ag_r.at[0], tp=tx),
-        remote(act.at[t], act.at[t], ag_s.at[1], ag_r.at[1], tp=ty),
-        remote(act.at[tx, pl.ds(0, mid)], act.at[tx, pl.ds(0, mid)], ag_s.at[2], ag_r.at[2], tp=ty),
-        remote(act.at[ty, pl.ds(mid, mid)], act.at[ty, pl.ds(mid, mid)], ag_s.at[3], ag_r.at[3],
-               tp=tx),
+        remote(act.at[of, at], act.at[of, at], ag_s.at[n], ag_r.at[n], tp=to)
+        for n, (of, at, to) in enumerate((
+            (t, low, tx), (t, high, ty), (t, high, tx), (t, low, ty), (tx, low, ty), (ty, high, tx),
+        ))
     ]
 
     def arrival(n, block):
@@ -260,17 +281,19 @@
     def columns(of):
         return ow[pl.ds(pl.multiple_of(of * ch, ch), ch), :]
 
-    ag[0].start()
-    ag[1].start()
+    for n in range(4):
+        ag[n].start()
     loads[0].wait()
     mixed[...] = res_ref[...].astype(F32) + dot(act[t], columns(t))
-    arrival(0, act.at[tx]).wait_recv()
-    ag[2].start()
-    arrival(1, act.at[ty]).wait_recv()
-    ag[3].start()
+    arrival(0, act.at[tx, low]).wait_recv()
+    ag[4].start()
+    arrival(1, act.at[ty, high]).wait_recv()
+    ag[5].start()
+    arrival(2, act.at[tx, high]).wait_recv()
+    arrival(3, act.at[ty, low]).wait_recv()
     mixed[...] += dot(act[tx], columns(tx)) + dot(act[ty], columns(ty))
-    arrival(2, act.at[td, pl.ds(0, mid)]).wait_recv()
-    arrival(3, act.at[td, pl.ds(mid, mid)]).wait_recv()
+    arrival(4, act.at[td, low]).wait_recv()
+    arrival(5, act.at[td, high]).wait_recv()
     full = mixed[...] + dot(act[td], columns(td))
     mixed[...] = full
     (sq,), st2 = row_totals(1, (jnp.sum(full * full, axis=1, keepdims=True),))
@@ -315,29 +338,35 @@
             place = k * size + (mi + i) % size
             remote(outgoing.at[piece(0)], arr.at[t, piece(place)], zs_s.at[0], zs_r.at[place],
                    sp=me).wait_recv()
-        own = arr.at[t, span(k)]
-        send(remote(own, own, x_s.at[4 * k], x_r.at[4 * k], tp=tx))
-        send(remote(own, own, x_s.at[4 * k + 1], x_r.at[4 * k + 1], tp=ty))
-
-    def landed(n, block):
-        remote(block, block, x_s.at[n], x_r.at[n], tp=tx).wait_recv()
+        pass_on(k, 0, t, front(k), tx)
+        pass_on(k, 1, t, rear(k), ty)
+        pass_on(k, 2, t, rear(k), tx)
+        pass_on(k, 3, t, front(k), ty)
+
+    def pass_on(k, n, of, at, to):
+        block = arr.at[of, at]
+        send(remote(block, block, x_s.at[6 * k + n], x_r.at[6 * k + n], tp=to))
+
+    def landed(k, n, of, at):
+        block = arr.at[of, at]
+        remote(block, block, x_s.at[6 * k + n], x_r.at[6 * k + n], tp=tx).wait_recv()
 
     def relay(k):
-        landed(4 * k, arr.at[tx, span(k)])
-        block = arr.at[tx, front(k)]
-        send(remote(block, block, x_s.at[4 * k + 2], x_r.at[4 * k + 2], tp=ty))
-        landed(4 * k + 1, arr.at[ty, span(k)])
-        block = arr.at[ty, rear(k)]
-        send(remote(block, block, x_s.at[4 * k + 3], x_r.at[4 * k + 3], tp=tx))
+        landed(k, 0, tx, front(k))
+        pass_on(k, 4, tx, front(k), ty)
+        landed(k, 1, ty, rear(k))
+        pass_on(k, 5, ty, rear(k), tx)
 
     def gather_end(k):
-        landed(4 * k + 2, arr.at[td, front(k)])
-        landed(4 * k + 3, arr.at[td, rear(k)])
+        landed(k, 2, tx, rear(k))
+        landed(k, 3, ty, front(k))
+        landed(k, 4, td, front(k))
+        landed(k, 5, td, rear(k))
 
     inner = wg.shape[1]
     tile = min(256, inner)
 
-    def experts(k):
+    def expert_up(k):
         def up(n, carry):
             at = pl.ds(pl.multiple_of(n * tile, tile), tile)
             g = jnp.zeros((grp, tile), F32)
@@ -349,15 +378,17 @@
             hid[:, at] = (jax.nn.silu(g) * u).astype(BF16)
             return carry
 
+        if k == 0:
+            loads[1].wait()
+            loads[2].wait()
+        lax.fori_loop(0, inner // tile, up, 0)
+
+    def expert_down(k):
         def down(b, carry):
             at = pl.ds(pl.multiple_of(b * ch, ch), ch)
             part[b, k * grp:(k + 1) * grp, :] = dot(hid[...], wd[:, at]).astype(BF16)
             return carry
 
-        if k == 0:
-            loads[1].wait()
-            loads[2].wait()
-        lax.fori_loop(0, inner // tile, up, 0)
         if k == 0:
             loads[3].wait()
         lax.fori_loop(0, ntp, down, 0)
@@ -401,28 +432,27 @@
             send(remote(fin.at[piece(k * size + who)], ret.at[piece(me)],
                         h_s.at[k * size + i], h_r.at[me], sp=home))
 
+    order = [(share, 0), (relay, 0), (share, 1)]
     for k in range(GROUPS):
-        if k == 0:
-            share(0)
-            share(1)
-        relay(k)
-        if 0 < k < GROUPS - 1:
-            share(k + 1)
-        gather_end(k)
-        experts(k)
+        order += [(gather_end, k), (expert_up, k)]
         if k >= 1:
-            reduce_mid(k - 1)
-        if k >= 2:
-            reduce_end(k - 2)
-    reduce_end(GROUPS - 2)
-    reduce_mid(GROUPS - 1)
-    reduce_end(GROUPS - 1)
+            order += [(reduce_mid, k - 1)]
+        if k + 1 < GROUPS:
+            order += [(relay, k + 1)]
+        order += [(expert_down, k)]
+        if k + 2 < GROUPS:
+            order += [(share, k + 2)]
+        if k >= 1:
+            order += [(reduce_end, k - 1)]
+    order += [(reduce_mid, GROUPS - 1), (reduce_end, GROUPS - 1)]
+    for step, k in order:
+        step(k)
 
     for d in range(1, nsp):
         e = (me + d) % nsp
         remote(fin.at[piece(0)], ret.at[piece(e)], h_s.at[0], h_r.at[e], sp=me).wait_recv()
     back = ret[...]
-    moe = dot(pick0, back) * rw_ref[:, 0:1] + dot(pick1, back) * rw_ref[:, 1:2]
+    moe = dot(pick0, back) * weights[:, 0:1] + dot(pick1, back) * weights[:, 1:2]
     out_ref[...] = (mixed[...] + moe).astype(out_ref.dtype)
 
     @pl.when(me < nsp - 1)
@@ -447,15 +477,18 @@
     slots = nsp * cap
     grp = slots // GROUPS
     edge = -(-(conv_weight.shape[0] // 2) // 16) * 16
+    small = [residual, glu_value, glu_gate, conv_weight]
+    small += [a.reshape(1, ch) for a in (conv_bias, ln_gain, ln_bias, norm_gain)]
+    small += [route_ids.T, route_weight.T]
     vmem = pl.BlockSpec(memory_space=pltpu.VMEM)
     hbm = pl.BlockSpec(memory_space=pl.ANY)
     dma = lambda n: pltpu.SemaphoreType.DMA((n,))
     return pl.pallas_call(
         functools.partial(layer_kernel, nsp, ntp),
         out_shape=jax.ShapeDtypeStruct((rows, ch), residual.dtype),
-        in_specs=[vmem] * 10 + [hbm] * 4,
+        in_specs=[hbm] * 14,
         out_specs=vmem,
-        scratch_shapes=[
+        scratch_shapes=[pltpu.VMEM(a.shape, a.dtype) for a in small] + [
             pltpu.VMEM((width, ch), BF16),
             pltpu.VMEM((width, inner), BF16),
             pltpu.VMEM((width, inner), BF16),
@@ -478,16 +511,14 @@
             pltpu.VMEM((slots, ch), BF16),
             pltpu.VMEM((slots, ch), BF16),
             pltpu.VMEM((slots, ch), BF16),
-            dma(4), dma(2), dma(2), dma(2 * ntp), dma(2 * ntp), dma(4), dma(4),
-            dma(nsp), dma(nsp), dma(4 * GROUPS), dma(4 * GROUPS), dma(6 * GROUPS),
+            dma(14), dma(2), dma(2), dma(2 * ntp), dma(2 * ntp), dma(6), dma(6),
+            dma(nsp), dma(nsp), dma(6 * GROUPS), dma(6 * GROUPS), dma(6 * GROUPS),
             dma(6 * GROUPS), dma(nsp), dma(nsp),
         ],
         compiler_params=pltpu.CompilerParams(
-            collective_id=0, has_side_effects=True, vmem_limit_bytes=52 * 1024 * 1024
+            collective_id=0, has_side_effects=True, vmem_limit_bytes=67043328
         ),
-    )(residual, glu_value, glu_gate, conv_weight, conv_bias.reshape(1, ch), ln_gain.reshape(1, ch),
-      ln_bias.reshape(1, ch), norm_gain.reshape(1, ch), route_ids, route_weight,
-      out_weight, expert_gate, expert_up, expert_down)
+    )(*small, out_weight, expert_gate, expert_up, expert_down)
 
 
 def solution(mesh):

time: 91.9 us -> 73.4 us (0.80)
  Pallas kernels: 82.9 us -> 71.7 us
  local copies, waits for them, and re-layouts: 8.41 us -> 1.57 us
    pallas_call x1, Pallas kernels: 82.9 us -> 71.7 us  [fused(): pl.pallas_call(functools.partial(layer_kernel, nsp, ntp), out_shape=jax.S...]
    unnamed x19 -> x1, local copies, waits for them, and re-layouts: 8.41 us -> 1.57 us
where the time goes in v2:
time: 73.4 us; the launch traced here: 73.3 us
  Pallas kernels  71.7 us (98%)
  local copies, waits for them, and re-layouts  1.57 us (2%)
    pallas_call x1, Pallas kernels, fused(): pl.pallas_call(functools.partial(layer_kernel, nsp, ntp), out_shape=jax.S...  71.7 us
    unnamed x1, local copies, waits for them, and re-layouts  1.57 us

profile of v2, /device:TPU:0, one launch (start us, length us, event | category | flops | bytes accessed | tf_op | source)
XLA Modules:
  0.0 73.3 jit_solution(18441982002566789651)
XLA Ops:
  0.0 71.7 %shard_map.136 = bf16[128,512]{1,0:T(8,128)(2,1)} custom-call(bf16[128,512]{1,0:T(8,128)(2,1)} %res_hbm.1, bf16[128,512]{1,0:T(8,128)(2,1)} %val_hbm.1, bf16[128,512]{1,0:T(8,128)(2,1)} %gate_hbm.1, bf16[31,512]{1,0:T(8,128)(2,1)} %cw_hbm.1, f32[1,512]{1,0:T(1,128)} %bitcast.6, f32[1,512]{1,0:T(1,128)} %bitcast.7, f32[1,512]{1,0:T(1,128)} %bitcast.8, ...), custom_call_target="tpu_custom_call" | custom-call | tf_op jit(solution)/shard_map/pallas_call | solution.py:486
  71.7 1.6 %copy.16 = bf16[128,512]{1,0:T(8,128)(2,1)} copy(bf16[128,512]{1,0:T(8,128)(2,1)} %shard_map.136) | data formatting | bytes 262144
